TPU v7x, 128 devices: a whole 4x4x4 slice. The times are simulated.
128 devices in a mesh: sp: 16 (over z, x), tp: 8 (over y, core).
Axes of the slice: x: 4, y: 4, z: 4, core: 2. Of those that a mesh axis runs over, the one named last changes fastest.
Arguments:
- query_small: bfloat16 [12288, 1024], P('sp', 'tp'), may hold values from -18 to 18
- key_small: bfloat16 [12288, 1024], P('sp', 'tp'), may hold values from -6 to 6
- value_small: bfloat16 [12288, 1024], P('sp', 'tp'), may hold values from -6 to 6
- offset_small: bfloat16 [16, 12288], P('tp', 'sp'), may hold values from -25 to 0
- query_large: bfloat16 [12288, 1024], P('sp', 'tp'), may hold values from -18 to 18
- key_large: bfloat16 [12288, 1024], P('sp', 'tp'), may hold values from -6 to 6
- value_large: bfloat16 [12288, 1024], P('sp', 'tp'), may hold values from -6 to 6
- offset_large: bfloat16 [8, 12288], P('tp', 'sp'), may hold values from -25 to 0
- out_small: bfloat16 [1024, 2048], P('tp'), may hold values from -0.125 to 0.125
- out_large: bfloat16 [1024, 2048], P('tp'), may hold values from -0.125 to 0.125
- residual: bfloat16 [12288, 2048], P(('sp', 'tp')), may hold values from -1.1953125 to 1.1953125
- norm_gain: bfloat16 [2048], replicated, may hold values from 0.099609375 to 1.8984375
- gate_weight: bfloat16 [2048, 5632], P('sp', 'tp'), may hold values from -0.125 to 0.125
- up_weight: bfloat16 [2048, 5632], P('sp', 'tp'), may hold values from -0.125 to 0.125
- down_weight: bfloat16 [5632, 2048], P('tp', 'sp'), may hold values from -0.078125 to 0.078125
Outputs:
- layer_out: bfloat16 [12288, 2048], P(('sp', 'tp'))
All inputs are finite; a program needn't handle non-finite values.
Results may differ from a plain program's by a relative error of at most 0.023.
Values may be sent and summed in bfloat16 or wider, within the bound.
No kernel may reach another device: no remote copies, remote signals or barrier semaphores. Data moves between devices by JAX's collectives and lax.ppermute only.
A program may use at most 128 MiB of HBM per device.

v0:
```python
import jax
import jax.numpy as jnp
from jax import lax
from jax.sharding import PartitionSpec as P

SMALL_DIM = 64
LARGE_DIM = 128


def turned_gather(arrays, axis, dims):
    turned = [jnp.moveaxis(a, dim, 0) for a, dim in zip(arrays, dims)]
    both = jnp.concatenate([t.reshape(len(t), -1) for t in turned], axis=1)
    whole, at, done = (lax.all_gather(both, axis, axis=0, tiled=True), 0, [])
    for t, dim in zip(turned, dims):
        share = whole[:, at : at + t[0].size].reshape(-1, *t.shape[1:])
        done.append(jnp.moveaxis(share, 0, dim))
        at += t[0].size
    return tuple(done)


def cut_along(value, dim, length):
    before, after = (value.shape[:dim], value.shape[dim + 1 :])
    return jnp.moveaxis(value.reshape(*before, length, -1, *after), dim, 0)


def summed_on_arrival(value, axis, dim):
    pieces = cut_along(value, dim, lax.axis_size(axis))
    arrived = lax.all_to_all(pieces, axis, split_axis=0, concat_axis=0, tiled=True)
    return arrived.astype(jnp.float32).sum(axis=0)


def split_heads(flat, head_depth):
    return flat.reshape(flat.shape[0], -1, head_depth)


def stick_terms(query, random_keys, values, offset, limits, carried):
    head_depth = query.shape[-1]
    key_heads = split_heads(random_keys, head_depth)
    value_heads = split_heads(values, head_depth)
    logits = jnp.einsum(
        "thd,shd->hts", query, key_heads, preferred_element_type=jnp.float32
    ) * head_depth ** (-0.5)
    logits = logits + offset.astype(jnp.float32)[:, None, :]
    fail_all = jax.nn.log_sigmoid(-logits)
    log_pass = logits + fail_all
    log_fail = fail_all
    before = None
    if limits is not None:
        query_first, key_first = limits
        query_pos = lax.broadcasted_iota(jnp.int32, logits.shape, 1) + query_first
        key_pos = lax.broadcasted_iota(jnp.int32, logits.shape, 2) + key_first
        before = key_pos < query_pos
        log_fail = jnp.where(before, fail_all, 0.0)
    suffix = lax.cumsum(log_fail, axis=2, reverse=True) - log_fail
    weights = jnp.exp(log_pass + suffix + carried[:, :, None])
    if before is not None:
        weights = jnp.where(before, weights, 0.0)
    weights = weights.astype(jnp.bfloat16)
    result = jnp.einsum("hts,shd->thd", weights, value_heads, preferred_element_type=jnp.float32)
    return (result, carried + jnp.sum(log_fail, axis=2))


def both_groups(queries, key_block, limits, totals):
    key_small, value_small, offset_small, key_large, value_large, offset_large = key_block
    out_small, acc_small, out_large, acc_large = totals
    term_small, next_small = stick_terms(
        queries[0], key_small, value_small, offset_small, limits, acc_small
    )
    term_large, next_large = stick_terms(
        queries[1], key_large, value_large, offset_large, limits, acc_large
    )
    return (out_small + term_small, next_small, out_large + term_large, next_large)


def empty_totals(rows, small_heads, large_heads):
    return (
        jnp.zeros((rows, small_heads, SMALL_DIM), jnp.float32),
        jnp.zeros((small_heads, rows), jnp.float32),
        jnp.zeros((rows, large_heads, LARGE_DIM), jnp.float32),
        jnp.zeros((large_heads, rows), jnp.float32),
    )


def rounded(value):
    return lax.optimization_barrier(value.astype(jnp.bfloat16)).astype(jnp.float32)


def rms_norm(stream, gain):
    scale = lax.rsqrt(jnp.mean(stream * stream, axis=-1, keepdims=True) + 1e-06)
    return (stream * scale * gain.astype(jnp.float32)).astype(jnp.bfloat16)


def on_device(
    query_small,
    key_small,
    value_small,
    offset_small,
    query_large,
    key_large,
    value_large,
    offset_large,
    out_small,
    out_large,
    residual,
    norm_gain,
    gate_weight,
    up_weight,
    down_weight,
):
    gate_full, up_full, down_full = turned_gather(
        (gate_weight, up_weight, down_weight), "sp", (0, 0, 1)
    )
    tokens = query_small.shape[0]
    small_heads = offset_small.shape[0]
    large_heads = offset_large.shape[0]
    queries = (split_heads(query_small, SMALL_DIM), split_heads(query_large, LARGE_DIM))
    own_block = (key_small, value_small, offset_small, key_large, value_large, offset_large)
    sp_index = lax.axis_index("sp")
    own_start = sp_index * tokens
    totals = both_groups(
        queries, own_block, (own_start, own_start), empty_totals(tokens, small_heads, large_heads)
    )
    key_dims = (0, 0, 1, 0, 0, 1)
    gathered = turned_gather(
        (own_block[0], own_block[1], own_block[2], own_block[3], own_block[4], own_block[5]),
        "sp",
        (0, 0, 1, 0, 0, 1),
    )

    def far_turn(turn_index, status):
        first_row = (sp_index - 1 - turn_index) * tokens
        key_block = tuple(
            (
                lax.dynamic_slice_in_dim(member, first_row, tokens, member_dim)
                for member, member_dim in zip(gathered, key_dims)
            )
        )
        return both_groups(queries, key_block, None, status)

    totals = lax.fori_loop(0, sp_index, far_turn, totals)
    mixed_small = totals[0].reshape(tokens, -1).astype(jnp.bfloat16)
    mixed_large = totals[2].reshape(tokens, -1).astype(jnp.bfloat16)
    attended = summed_on_arrival(
        (
            jnp.dot(mixed_small, out_small, preferred_element_type=jnp.float32)
            + jnp.dot(mixed_large, out_large, preferred_element_type=jnp.float32)
        ).astype(jnp.bfloat16),
        "tp",
        0,
    )
    stream = residual.astype(jnp.float32) + rounded(attended)
    normed = rms_norm(stream, norm_gain)
    normed_rows = lax.all_gather(normed, "tp", axis=0, tiled=True)
    gate = jnp.dot(normed_rows, gate_full, preferred_element_type=jnp.float32)
    upper = jnp.dot(normed_rows, up_full, preferred_element_type=jnp.float32)
    hidden = (jax.nn.silu(gate) * upper).astype(jnp.bfloat16)
    summed = lax.psum_scatter(
        jnp.dot(hidden, down_full, preferred_element_type=jnp.float32).astype(jnp.bfloat16),
        "tp",
        scatter_dimension=0,
        tiled=True,
    ).astype(jnp.float32)
    return (stream + rounded(summed)).astype(jnp.bfloat16)


def solution(mesh):
    return jax.shard_map(
        on_device,
        mesh=mesh,
        in_specs=(
            P("sp", "tp"),
            P("sp", "tp"),
            P("sp", "tp"),
            P("tp", "sp"),
            P("sp", "tp"),
            P("sp", "tp"),
            P("sp", "tp"),
            P("tp", "sp"),
            P("tp", None),
            P("tp", None),
            P(("sp", "tp"), None),
            P(),
            P("sp", "tp"),
            P("sp", "tp"),
            P("tp", "sp"),
        ),
        out_specs=P(("sp", "tp"), None),
        check_vma=False,
    )
```

profile of v0, /device:TPU:0, one launch (start us, length us, event | category | flops | bytes accessed | tf_op | source)
XLA Modules:
  0.0 1112.9 jit_solution(5923392795557188407)
XLA Ops:
  6.6 0.0 all-gather.4.cloned.1.call-start
  6.7 1.0 copy.47
  7.6 0.9 copy.48
  8.5 3.2 concatenate.6
  11.7 0.0 all-gather.4.cloned.1.call-update
  11.7 0.0 all-gather.8.cloned.1.call-start
  11.8 0.8 pad_maximum_fusion
  12.7 0.1 copy.40
  12.8 0.8 copy.43
  13.7 3.2 fusion.59
  17.0 7.9 fusion.38
  24.9 2.2 copy.46
  27.1 0.8 copy.39
  28.0 2.4 fusion.54
  30.4 3.9 fusion.60
  34.4 15.1 %fusion.33 = f32[2,768,6,128]{1,2,3,0:T(8,128)S(1)} fusion(f32[2,768,6,128]{1,3,2,0:T(8,128)S(1)} %bitcast.216), kind=kOutput, calls=%fused_computation.58 | output fusion | flops 149815296 | bytes 9437184 | tf_op jit(solution)/shard_map/reduce-window.4
  49.5 2.7 copy-done.4
  52.3 0.1 reduce-window.49
  52.3 4.7 broadcast_add_fusion.1
  57.1 1.4 copy.42
  58.5 0.9 copy-done.3
  59.4 0.1 copy-done.12
  59.5 18.9 %fusion.35 = bf16[2,768,768]{1,2,0:T(8,128)(2,1)S(1)} fusion(f32[2,768,768]{1,2,0:T(8,128)S(1)} %copy-done.3, f32[2,768,6,128]{1,3,2,0:T(8,128)S(1)} %copy.42, f32[2,768,768]{1,2,0:T(8,128)S(1)} %bitcast.219, f32[2,768]{1,0:T(2,128)S(1)} %convert_element_type.74, s32[768]{0:T(1024)S(1)} %iota_add_fusion, u8[768,768]{0,1:T(8,128)(4,1)S(1)} %copy-done.12), kind=kLoop, calls=%fused_computation.63 | loop fusion | flops 21233664 | bytes 17114112 | tf_op jit(solution)/shard_map/convert_element_type | solution.py:58
  78.5 5.6 fusion.45
  84.2 1.1 convolution_bitcast_fusion.3
  85.3 1.3 convolution_bitcast_fusion.2
  86.6 33.8 %all-gather.4.cloned.1.call-done = bf16[12288,515]{1,0:T(8,128)(2,1)} async-done(((bf16[768,515]{1,0:T(8,128)(2,1)}), bf16[12288,515]{1,0:T(8,128)(2,1)}) %all-gather.4.cloned.1.call-update) | async-done | bytes 12656656 | tf_op jit(solution)/shard_map/all_gather | solution.py:13
  120.3 3.2 slice_bitcast_fusion.3
  123.6 3.2 copy.52
  126.8 3.5 slice_reduce_fusion
  130.4 12.6 %fusion.61 = (bf16[12288,128]{1,0:T(8,128)(2,1)}, bf16[12288,128]{1,0:T(8,128)(2,1)}, bf16[12288,128]{1,0:T(8,128)(2,1)}, bf16[12288,128]{1,0:T(8,128)(2,1)}) fusion(bf16[12288,515]{1,0:T(8,128)(2,1)} %all-gather.4.cloned.1.call-done), kind=kLoop, calls=%fused_computation.112 | loop fusion | bytes 25165824 | tf_op jit(solution)/shard_map/slice | solution.py:15
  143.0 1.0 convert_element_type.77
  144.0 1.0 fusion.62
  145.0 0.1 copy-done.17
  145.2 2.7 add_convert_fusion
  147.9 4.6 all-to-all-start
  152.5 0.0 all-gather.6.cloned.1.call-start
  152.5 38.3 %all-to-all-done = bf16[8,96,2048]{2,1,0:T(8,128)(2,1)} async-done(((bf16[8,96,2048]{2,1,0:T(8,128)(2,1)}), bf16[8,96,2048]{2,1,0:T(8,128)(2,1)}, u32[]{:S(2)}, u32[]{:S(2)}) %all-to-all-start) | async-done | bytes 3145760 | tf_op jit(solution)/shard_map/all_to_all | solution.py:28
  190.9 2.6 reduce_sum.64
  193.5 0.2 multiply_reduce_fusion
  193.7 0.9 multiply_convert_fusion.1
  194.7 0.0 reduce-scatter.2.cloned.1.call-start
  194.7 6.0 all-gather.8.cloned.1.call-done
  200.7 850.4 %all-gather.6.cloned.1.call-done = bf16[768,2048]{1,0:T(8,128)(2,1)} async-done(((bf16[96,2048]{1,0:T(8,128)(2,1)}), bf16[768,2048]{1,0:T(8,128)(2,1)}) %all-gather.6.cloned.1.call-update) | async-done | bytes 3145744 | tf_op jit(solution)/shard_map/all_gather | solution.py:153
  1051.1 5.2 fusion.43
  1056.3 11.8 %convolution_convert_fusion = bf16[768,2048]{1,0:T(8,128)(2,1)} fusion(bf16[2048,2112]{0,1:T(8,128)(2,1)} %all-gather.8.cloned.1.call-done, f32[768,704]{0,1:T(8,128)S(1)} %fusion.43, bf16[768,2048]{1,0:T(8,128)(2,1)} %all-gather.6.cloned.1.call-done), kind=kOutput, calls=%fused_computation.71 | convolution fusion | flops 4434001920 | bytes 14221312 | tf_op jit(solution)/shard_map/dot_general | solution.py:158
  1068.2 36.1 %reduce-scatter.2.cloned.1.call-done = bf16[96,2048]{1,0:T(8,128)(2,1)} async-done(((bf16[768,2048]{1,0:T(8,128)(2,1)}), bf16[96,2048]{1,0:T(8,128)(2,1)}) %reduce-scatter.2.cloned.1.call-update) | async-done | bytes 393232 | tf_op jit(solution)/shard_map/reduce_scatter | solution.py:157
  1104.2 1.9 add_convert_fusion.1
  (65 shorter events, 0.3 us)
Async XLA Ops:
  6.5 137.5 %copy-start = (bf16[128,2048]{1,0:T(8,128)(2,1)S(1)}, bf16[128,2048]{1,0:T(8,128)(2,1)}, u32[]{:S(2)}) copy-start(bf16[128,2048]{1,0:T(8,128)(2,1)} %param.25) | copy-start | bytes 1572868
  6.5 6.1 copy-start.24
  6.5 7.1 copy-start.23
  6.5 6.1 copy-start.14
  6.5 6.3 copy-start.15
  6.6 7.2 copy-start.18
  6.6 5.2 copy-start.20
  6.6 5.2 copy-start.22
  6.6 5.2 copy-start.21
  6.6 7.1 copy-start.26
  6.6 113.7 %all-gather.4.cloned.1.call-start = ((), (), s32[]{:S(2)}) async-start(), calls=%async_computation.2 | async-start | bytes 16711680 | tf_op jit(solution)/shard_map/all_gather | solution.py:13
  11.7 189.0 %all-gather.8.cloned.1.call-start = ((), (), s32[]{:S(2)}) async-start(), calls=%async_computation.4 | async-start | bytes 9191424 | tf_op jit(solution)/shard_map/all_gather | solution.py:13
  17.0 10.2 copy-start.9
  24.9 2.2 copy-start.19
  30.4 4.0 copy-start.8
  30.4 4.0 copy-start.11
  34.3 15.2 %copy-start.2 = (f32[2,768,768]{1,2,0:T(8,128)}, f32[2,768,768]{1,2,0:T(8,128)S(1)}, u32[]{:S(2)}) copy-start(f32[2,768,768]{1,2,0:T(8,128)S(1)} %get-tuple-element.239) | copy-start | bytes 14155780
  34.4 24.1 %slice-start.2 = ((s8[4718592]{0:T(1024)(128)(4,1)}), s8[524288]{0:T(1024)(128)(4,1)S(1)}, s32[]{:S(2)}) async-start(s8[4718592]{0:T(1024)(128)(4,1)} %bitcast.218), calls=%async_computation.8 | async-start | bytes 1048576
  49.5 2.7 copy-start.4
  52.3 6.1 slice-start.3
  57.0 2.3 copy-start.3
  57.0 2.5 copy-start.12
  78.5 5.6 copy-start.13
  78.5 6.7 copy-start.16
  144.0 1.0 copy-start.7
  144.0 1.2 copy-start.17
  147.9 4.6 copy-start.25
  147.9 43.0 %all-to-all-start = ((bf16[8,96,2048]{2,1,0:T(8,128)(2,1)}), bf16[8,96,2048]{2,1,0:T(8,128)(2,1)}, u32[]{:S(2)}, u32[]{:S(2)}) async-start(bf16[8,96,2048]{2,1,0:T(8,128)(2,1)} %bitcast.220), calls=%async_computation | async-start | bytes 6291456 | tf_op jit(solution)/shard_map/all_to_all | solution.py:28
  152.5 41.0 %copy-start.10 = (bf16[96,2048]{1,0:T(8,128)(2,1)S(1)}, bf16[96,2048]{1,0:T(8,128)(2,1)}, u32[]{:S(2)}) copy-start(bf16[96,2048]{1,0:T(8,128)(2,1)} %param.27) | copy-start | bytes 1179652
  152.5 898.7 %all-gather.6.cloned.1.call-start = ((), (), s32[]{:S(2)}) async-start(), calls=%async_computation.3 | async-start | bytes 3538944 | tf_op jit(solution)/shard_map/all_gather | solution.py:153
  194.7 909.6 %reduce-scatter.2.cloned.1.call-start = ((), (), s32[]{:S(2)}) async-start(), calls=%async_computation.5 | async-start | bytes 3538944 | tf_op jit(solution)/shard_map/reduce_scatter | solution.py:157
Sparse Core Ops, SparseCore 0:
  11.8 108.4 all-gather.3
  122.4 78.2 all-gather.7
  202.4 848.6 all-gather.5
  1068.3 35.9 reduce-scatter.1
where the time goes:
time: 1120 us; the launch traced here: 1110 us
  waiting for transfers between devices  965 us (86%)
  other arithmetic  63.8 us (6%)
  local copies, waits for them, and re-layouts  37.1 us (3%)
  matrix products  28.8 us (3%)
  between operations  13.8 us (1%)
    all_gather x1, waiting for transfers between devices, on_device(): normed_rows = lax.all_gather(normed, 'tp', axis=0, tiled=True)  850 us
    all_gather x2, waiting for transfers between devices, turned_gather(): whole, at, done = (lax.all_gather(both, axis, axis=0, tiled=True), 0, [])  39.8 us
    all_to_all x1, waiting for transfers between devices, summed_on_arrival(): lax.all_to_all(pieces, axis, split_axis=0, concat_axis=0, tiled=True)  38.3 us
    reduce_scatter x1, waiting for transfers between devices, on_device(): lax.psum_scatter(jnp.dot(hidden, down_full, preferred_element_type=jnp.fl...  36.1 us
    convert_element_type x2, other arithmetic, stick_terms(): weights = weights.astype(jnp.bfloat16)  24.5 us
    another operation x4, other arithmetic  23.2 us
  transfers between devices with their start and end apart: 5, of which 5 were waited for; matrix products, arithmetic and copies ran while one was open for 9% of the time, Pallas kernels for 0%

commit v1 on v0

--- a/solution.py
+++ b/solution.py
@@ -2,9 +2,31 @@
 import jax.numpy as jnp
 from jax import lax
 from jax.sharding import PartitionSpec as P
+from jax.lax import axis_index, axis_size, ppermute
 
 SMALL_DIM = 64
 LARGE_DIM = 128
+
+
+def follow_task(x0):
+    far_arr, b_now, local_now = (axis_size("tp"), axis_index("tp"), x0.shape[0])
+    kept_rows = list(map(lambda dev: (dev, (dev + 1) % far_arr), range(far_arr)))
+    store = list(map(lambda dev: (dev, (dev - 1) % far_arr), range(far_arr)))
+    answer = jnp.zeros((*x0.shape[:0], far_arr * local_now, *x0.shape[1:]), x0.dtype)
+    answer = lax.dynamic_update_slice_in_dim(answer, x0, b_now * local_now, axis=0)
+    r1 = r_now = x0
+    aux = far_arr // 2
+    for w in range(1, aux + 1):
+        r1 = ppermute(r1, "tp", kept_rows)
+        answer = lax.dynamic_update_slice_in_dim(
+            answer, r1, (b_now - w) % far_arr * local_now, axis=0
+        )
+        if w < far_arr - aux:
+            r_now = ppermute(r_now, "tp", store)
+            answer = lax.dynamic_update_slice_in_dim(
+                answer, r_now, (b_now + w) % far_arr * local_now, axis=0
+            )
+    return answer
 
 
 def turned_gather(arrays, axis, dims):
@@ -150,7 +172,7 @@
     )
     stream = residual.astype(jnp.float32) + rounded(attended)
     normed = rms_norm(stream, norm_gain)
-    normed_rows = lax.all_gather(normed, "tp", axis=0, tiled=True)
+    normed_rows = follow_task(normed)
     gate = jnp.dot(normed_rows, gate_full, preferred_element_type=jnp.float32)
     upper = jnp.dot(normed_rows, up_full, preferred_element_type=jnp.float32)
     hidden = (jax.nn.silu(gate) * upper).astype(jnp.bfloat16)

time: 1120 us -> 1130 us (level)
    all_gather x1 -> x0, waiting for transfers between devices: 850 us -> none  [on_device(): normed_rows = lax.all_gather(normed, 'tp', axis=0, tiled=True)]
    reduce_scatter x1, waiting for transfers between devices: 36.1 us -> 864 us  [on_device(): lax.psum_scatter(jnp.dot(hidden, down_full, preferred_element_type=jnp.fl...]
    ppermute x0 -> x7, waiting for transfers between devices: none -> 20.1 us  [the longest x4 20.1 us: follow_task(): r1 = ppermute(r1, 'tp', kept_rows)]
  transfers between devices with their start and end apart: 5 -> 11, of which waited for: 5 -> 7; matrix products, arithmetic and copies ran while one was open for 9% -> 10% of each run, Pallas kernels for 0% -> 0%
where the time goes in v1:
time: 1130 us; the launch traced here: 1120 us
  waiting for transfers between devices  956 us (85%)
  other arithmetic  63.9 us (6%)
  local copies, waits for them, and re-layouts  44.7 us (4%)
  matrix products  28.7 us (3%)
  between operations  13.8 us (1%)
  starting transfers between devices  13.6 us (1%)
    reduce_scatter x1, waiting for transfers between devices, on_device(): lax.psum_scatter(jnp.dot(hidden, down_full, preferred_element_type=jnp.fl...  864 us
    all_to_all x1, waiting for transfers between devices, summed_on_arrival(): lax.all_to_all(pieces, axis, split_axis=0, concat_axis=0, tiled=True)  38.3 us
    all_gather x2, waiting for transfers between devices, turned_gather(): whole, at, done = (lax.all_gather(both, axis, axis=0, tiled=True), 0, [])  33.8 us
    convert_element_type x2, other arithmetic, stick_terms(): weights = weights.astype(jnp.bfloat16)  24.5 us
    another operation x4, other arithmetic  23.2 us
  transfers between devices with their start and end apart: 11, of which 7 were waited for; matrix products, arithmetic and copies ran while one was open for 10% of the time, Pallas kernels for 0%

profile of v1, /device:TPU:0, one launch (start us, length us, event | category | flops | bytes accessed | tf_op | source)
XLA Modules:
  0.0 1121.0 jit_solution(922381284366145240)
XLA Ops:
  6.7 1.0 copy.47
  7.6 0.9 copy.48
  8.5 3.2 concatenate.6
  11.8 0.9 pad_maximum_fusion
  12.9 0.8 copy.43
  13.7 3.3 fusion.59
  17.0 7.9 fusion.38
  24.9 2.2 copy.46
  27.1 0.8 copy.39
  28.0 2.4 fusion.50
  30.4 3.9 fusion.60
  34.4 15.1 %fusion.33 = f32[2,768,6,128]{1,2,3,0:T(8,128)S(1)} fusion(f32[2,768,6,128]{1,3,2,0:T(8,128)S(1)} %bitcast.216), kind=kOutput, calls=%fused_computation.58 | output fusion | flops 149815296 | bytes 9437184 | tf_op jit(solution)/shard_map/reduce-window.4
  49.5 2.7 copy-done.4
  52.4 4.7 broadcast_add_fusion.1
  57.1 1.4 copy.42
  58.5 0.9 copy-done.3
  59.5 18.9 %fusion.35 = bf16[2,768,768]{1,2,0:T(8,128)(2,1)S(1)} fusion(f32[2,768,768]{1,2,0:T(8,128)S(1)} %copy-done.3, f32[2,768,6,128]{1,3,2,0:T(8,128)S(1)} %copy.42, f32[2,768,768]{1,2,0:T(8,128)S(1)} %bitcast.219, f32[2,768]{1,0:T(2,128)S(1)} %convert_element_type.74, s32[768]{0:T(1024)S(1)} %iota_add_fusion, u8[768,768]{0,1:T(8,128)(4,1)S(1)} %copy-done.12), kind=kLoop, calls=%fused_computation.63 | loop fusion | flops 21233664 | bytes 17114112 | tf_op jit(solution)/shard_map/convert_element_type | solution.py:80
  78.5 5.6 fusion.45
  84.2 1.1 convolution_bitcast_fusion.3
  85.3 1.3 convolution_bitcast_fusion.2
  86.6 33.7 %all-gather.3.cloned.1.call-done = bf16[12288,515]{1,0:T(8,128)(2,1)} async-done(((bf16[768,515]{1,0:T(8,128)(2,1)}), bf16[12288,515]{1,0:T(8,128)(2,1)}) %all-gather.3.cloned.1.call-update) | async-done | bytes 12656656 | tf_op jit(solution)/shard_map/all_gather | solution.py:35
  120.3 3.2 slice_bitcast_fusion.3
  123.6 3.2 copy.52
  126.8 3.6 slice_reduce_fusion
  130.4 12.6 %fusion.61 = (bf16[12288,128]{1,0:T(8,128)(2,1)}, bf16[12288,128]{1,0:T(8,128)(2,1)}, bf16[12288,128]{1,0:T(8,128)(2,1)}, bf16[12288,128]{1,0:T(8,128)(2,1)}) fusion(bf16[12288,515]{1,0:T(8,128)(2,1)} %all-gather.3.cloned.1.call-done), kind=kLoop, calls=%fused_computation.120 | loop fusion | bytes 25165824 | tf_op jit(solution)/shard_map/slice | solution.py:37
  143.0 1.0 convert_element_type.77
  144.0 1.0 fusion.62
  145.2 2.7 add_convert_fusion
  147.9 4.6 all-to-all-start
  152.5 38.3 %all-to-all-done = bf16[8,96,2048]{2,1,0:T(8,128)(2,1)} async-done(((bf16[8,96,2048]{2,1,0:T(8,128)(2,1)}), bf16[8,96,2048]{2,1,0:T(8,128)(2,1)}, u32[]{:S(2)}, u32[]{:S(2)}) %all-to-all-start) | async-done | bytes 3145760 | tf_op jit(solution)/shard_map/all_to_all | solution.py:50
  190.9 2.6 reduce_sum.64
  193.7 2.1 broadcast_in_dim.8
  195.8 0.9 constant_dynamic-update-slice_fusion.7
  196.7 3.0 collective-permute-start.1
  199.7 5.5 collective-permute-done
  205.1 3.0 collective-permute-start.3
  209.6 3.9 collective-permute-done.2
  213.6 3.0 collective-permute-start.5
  216.5 0.8 constant_dynamic-update-slice_fusion.4
  218.1 3.9 collective-permute-done.4
  222.0 0.8 constant_dynamic-update-slice_fusion.2
  222.8 0.8 constant_dynamic-update-slice_fusion.1
  223.6 6.8 collective-permute-done.6
  230.4 0.8 constant_dynamic-update-slice_fusion
  231.2 5.2 fusion.41
  236.4 11.8 %convolution_convert_fusion = bf16[768,2048]{1,0:T(8,128)(2,1)} fusion(bf16[2048,2112]{0,1:T(8,128)(2,1)} %all-gather.5.cloned.1.call-done, f32[768,704]{0,1:T(8,128)S(1)} %fusion.41, bf16[768,2048]{1,0:T(8,128)(2,1)} %constant_dynamic-update-slice_fusion), kind=kOutput, calls=%fused_computation.71 | convolution fusion | flops 4434001920 | bytes 14221312 | tf_op jit(solution)/shard_map/dot_general | solution.py:180
  248.2 864.2 %reduce-scatter.2.cloned.1.call-done = bf16[96,2048]{1,0:T(8,128)(2,1)} async-done(((bf16[768,2048]{1,0:T(8,128)(2,1)}), bf16[96,2048]{1,0:T(8,128)(2,1)}) %reduce-scatter.2.cloned.1.call-update) | async-done | bytes 393232 | tf_op jit(solution)/shard_map/reduce_scatter | solution.py:179
  1112.4 1.9 add_convert_fusion.1
  (84 shorter events, 3.5 us)
Async XLA Ops:
  6.5 137.5 %copy-start = (bf16[128,2048]{1,0:T(8,128)(2,1)S(1)}, bf16[128,2048]{1,0:T(8,128)(2,1)}, u32[]{:S(2)}) copy-start(bf16[128,2048]{1,0:T(8,128)(2,1)} %param.25) | copy-start | bytes 1572868
  6.5 6.1 copy-start.24
  6.5 7.1 copy-start.23
  6.5 6.1 copy-start.14
  6.5 6.3 copy-start.15
  6.6 7.2 copy-start.18
  6.6 5.2 copy-start.20
  6.6 5.2 copy-start.22
  6.6 5.2 copy-start.21
  6.6 7.1 copy-start.26
  6.6 113.7 %all-gather.3.cloned.1.call-start = ((), (), s32[]{:S(2)}) async-start(), calls=%async_computation.2 | async-start | bytes 16711680 | tf_op jit(solution)/shard_map/all_gather | solution.py:35
  11.7 219.5 %all-gather.5.cloned.1.call-start = ((), (), s32[]{:S(2)}) async-start(), calls=%async_computation.3 | async-start | bytes 9191424 | tf_op jit(solution)/shard_map/all_gather | solution.py:35
  17.0 10.1 copy-start.9
  24.9 2.2 copy-start.19
  30.4 4.0 copy-start.8
  30.4 4.0 copy-start.11
  34.4 15.2 %copy-start.2 = (f32[2,768,768]{1,2,0:T(8,128)}, f32[2,768,768]{1,2,0:T(8,128)S(1)}, u32[]{:S(2)}) copy-start(f32[2,768,768]{1,2,0:T(8,128)S(1)} %get-tuple-element.241) | copy-start | bytes 14155780
  34.4 24.1 %slice-start.2 = ((s8[4718592]{0:T(1024)(128)(4,1)}), s8[524288]{0:T(1024)(128)(4,1)S(1)}, s32[]{:S(2)}) async-start(s8[4718592]{0:T(1024)(128)(4,1)} %bitcast.218), calls=%async_computation.7 | async-start | bytes 1048576
  49.5 2.7 copy-start.4
  52.3 6.1 slice-start.3
  57.0 2.3 copy-start.3
  57.0 2.5 copy-start.12
  78.5 5.6 copy-start.13
  78.5 6.8 copy-start.16
  144.0 1.0 copy-start.7
  144.0 1.2 copy-start.17
  147.9 4.7 copy-start.25
  147.9 43.0 %all-to-all-start = ((bf16[8,96,2048]{2,1,0:T(8,128)(2,1)}), bf16[8,96,2048]{2,1,0:T(8,128)(2,1)}, u32[]{:S(2)}, u32[]{:S(2)}) async-start(bf16[8,96,2048]{2,1,0:T(8,128)(2,1)} %bitcast.220), calls=%async_computation | async-start | bytes 6291456 | tf_op jit(solution)/shard_map/all_to_all | solution.py:50
  152.5 41.0 %copy-start.10 = (bf16[96,2048]{1,0:T(8,128)(2,1)S(1)}, bf16[96,2048]{1,0:T(8,128)(2,1)}, u32[]{:S(2)}) copy-start(bf16[96,2048]{1,0:T(8,128)(2,1)} %param.27) | copy-start | bytes 1179652
  152.5 959.9 %reduce-scatter.2.cloned.1.call-start = ((), (), s32[]{:S(2)}) async-start(), calls=%async_computation.4 | async-start | bytes 3538944 | tf_op jit(solution)/shard_map/reduce_scatter | solution.py:179
  196.7 8.4 collective-permute-start
  196.7 8.4 collective-permute-start.1
  205.1 8.4 collective-permute-start.2
  205.1 8.4 collective-permute-start.3
  213.6 8.4 collective-permute-start.4
  213.6 9.2 collective-permute-start.5
  222.0 8.4 collective-permute-start.6
Sparse Core Ops, SparseCore 0:
  11.8 108.4 all-gather.2
  122.4 78.2 all-gather.4
  248.3 864.0 reduce-scatter.1
